TPU v7x, 512 devices: a whole 4x4x16 slice. The times are simulated.
512 devices in a mesh: kv: 128 (over z, x, core), tp: 4 (over y).
Axes of the slice: x: 4, y: 4, z: 16, core: 2. Of those that a mesh axis runs over, the one named last changes fastest.
Arguments:
- tokens: bfloat16 [65536, 2048], P(('kv', 'tp')), may hold values from -6 to 6
- query_weight: bfloat16 [2048, 1024], P(None, 'tp'), may hold values from -0.125 to 0.125
- latent_weight: bfloat16 [2048, 256], replicated, may hold values from -0.125 to 0.125
- key_absorb: bfloat16 [8, 128, 256], P('tp'), may hold values from -0.5 to 0.5
- query_gain: bfloat16 [256], replicated, may hold values from 0.4 to 8
- latent_gain: bfloat16 [256], replicated, may hold values from 0.4 to 8
- value_absorb: bfloat16 [8, 256, 128], P('tp'), may hold values from -0.375 to 0.375
- head_gain: bfloat16 [8, 128], P('tp'), may hold values from 0.099609375 to 1.8984375
- out_weight: bfloat16 [1024, 2048], P('tp'), may hold values from -0.1875 to 0.1875
- chosen: int32 [1024, 16], P('kv'), may hold values from 0 to 1023, as said below
Outputs:
- mixed_out: bfloat16 [65536, 2048], P(('kv', 'tp'))
Inputs may be any that keep to these rules, and one draw needn't show every extreme that they name: `chosen`: entry 0 of row b is b; a row's entries are distinct. Entries 1 to 3 lie in the same aligned run of 8 block numbers as b, the other 12 in other runs. For each aligned run of 8 rows and each other aligned run of 8 block numbers, those rows together name at most one block of that run. Entries above the row's own number may occur and contribute nothing.
All inputs are finite; a program needn't handle non-finite values.
Results may differ from a plain program's by a relative error of at most 0.014.
The roundings to bfloat16 on the way count: a program that leaves them out, or rounds other values in their place, can miss the bound.
Values may be sent and summed in bfloat16 or wider, within the bound.
A program may use at most 64 MiB of HBM per device.

v0:
```python
import jax
import jax.numpy as jnp
from jax import lax
from jax.sharding import Mesh
from jax.sharding import PartitionSpec as P

KV = ("kv_0", "kv_1", "kv_2")
KV_TP = ("kv_0", "kv_1", "kv_2", "tp")


epsilon = 1e-06


def cut_along(x, dim, peers):
    before, after = (x.shape[:dim], x.shape[dim + 1 :])
    return jnp.moveaxis(x.reshape(*before, peers, -1, *after), dim, 0)


def laid_out(blocks, dim):
    blocks = jnp.moveaxis(blocks, 0, dim)
    dims = blocks.shape
    return blocks.reshape(*dims[:dim], dims[dim] * dims[dim + 1], *dims[dim + 2 :])


def moved_by_axis(blocks, axes, turns):
    inside = blocks.shape[1:]
    filled = blocks.reshape(*(lax.axis_size(a) for a in axes), *inside)
    for k in turns:
        filled = lax.all_to_all(filled, axes[k], k, k, tiled=True)
    return filled.reshape(-1, *inside)


def core_and_chips(x, groups, turns, split_dim, concat_dim):
    peers = lax.axis_size(groups[0]) * lax.axis_size(groups[1])
    blocks = cut_along(x, split_dim, peers)
    return laid_out(moved_by_axis(blocks, groups, turns), concat_dim)


def copy_for_each(x, axis):
    copies = jnp.broadcast_to(x, (lax.axis_size(axis), *x.shape))
    return lax.all_to_all(copies, axis, split_axis=0, concat_axis=0, tiled=True)


def collect(x, axis, dim):
    blocks = copy_for_each(x, axis)
    return laid_out(blocks, dim)


def summed_on_arrival(x, axis, dim):
    blocks = cut_along(x, dim, lax.axis_size(axis))
    arrived = lax.all_to_all(blocks, axis, split_axis=0, concat_axis=0, tiled=True)
    return arrived.astype(jnp.float32).sum(axis=0)


def normalize(values, gain):
    return values * lax.rsqrt(jnp.mean(values * values, axis=-1, keepdims=True) + epsilon) * gain


def body(
    tokens,
    query_weight,
    latent_weight,
    key_absorb,
    query_gain,
    latent_gain,
    value_absorb,
    head_gain,
    out_weight,
    chosen,
):
    width_query = query_weight.shape[1]
    shard_rows = lax.all_gather(tokens, "tp", axis=0, tiled=True)
    query_part = jnp.dot(shard_rows, query_weight, preferred_element_type=jnp.float32)
    latent_part = jnp.dot(shard_rows, latent_weight, preferred_element_type=jnp.float32)
    projected = jnp.concatenate([query_part, latent_part], axis=1)
    local_heads, head_width, latent_width = key_absorb.shape
    span_tokens = projected.shape[0]
    queries = (
        projected[:, :width_query]
        .astype(jnp.bfloat16)
        .reshape(span_tokens, local_heads, head_width)
    )
    latent = normalize(projected[:, width_query:], latent_gain.astype(jnp.float32)).astype(
        jnp.bfloat16
    )
    absorbed = jnp.einsum("thd,hdc->thc", queries, key_absorb, preferred_element_type=jnp.float32)
    absorbed = normalize(absorbed, query_gain.astype(jnp.float32)).astype(jnp.bfloat16)
    block_count, pick_count = chosen.shape
    block_len = span_tokens // block_count
    devices = lax.axis_size(KV)
    own_index = lax.axis_index(KV)
    owner_of = chosen // block_count
    within = chosen % block_count
    device_ids = jnp.arange(devices, dtype=jnp.int32)
    matches = owner_of[:, :, None] == device_ids[None, None, :]
    wanted = jnp.max(jnp.where(matches, within[:, :, None], 0), axis=(0, 1))
    asked_for = core_and_chips(wanted, (("kv_0", "kv_1"), "kv_2"), (1, 0), 0, 0)
    blocks = latent.reshape(block_count, block_len, latent_width)
    share_len = block_len // lax.axis_size("tp")
    row_share = lax.dynamic_slice_in_dim(blocks, lax.axis_index("tp") * share_len, share_len, 1)
    outgoing = jnp.take(row_share, asked_for, axis=0)
    share_rows = lax.all_to_all(outgoing, KV, split_axis=0, concat_axis=0, tiled=True)
    arrived = collect(share_rows, "tp", 1)
    key_table = jnp.concatenate([blocks, arrived], axis=0)
    table_slot = jnp.where(owner_of == own_index, within, block_count + owner_of)
    key_rows = jnp.take(key_table, table_slot, axis=0).reshape(
        block_count, pick_count * block_len, latent_width
    )
    offsets = jnp.arange(block_len, dtype=jnp.int32)
    key_pos = (chosen[:, :, None] * block_len + offsets[None, None, :]).reshape(
        block_count, pick_count * block_len
    )
    block_ids = own_index * block_count + jnp.arange(block_count, dtype=jnp.int32)
    query_pos = block_ids[:, None] * block_len + offsets[None, :]
    visible = key_pos[:, None, :] <= query_pos[:, :, None]
    grouped = absorbed.reshape(block_count, block_len, local_heads, latent_width)
    scores = jnp.einsum(
        "bqhc,bkc->bhqk", grouped, key_rows, preferred_element_type=jnp.float32
    ) * latent_width ** (-0.5)
    scores = jnp.where(visible[:, None], scores, -jnp.inf)
    weights = jax.nn.softmax(scores, axis=-1).astype(jnp.bfloat16)
    mixed = jnp.einsum(
        "bhqk,bkc->bqhc", weights, key_rows, preferred_element_type=jnp.float32
    ).astype(jnp.bfloat16)
    mixed = mixed.reshape(span_tokens, local_heads, latent_width)
    values = jnp.einsum("thc,hcd->thd", mixed, value_absorb, preferred_element_type=jnp.float32)
    head_out = (
        normalize(values, head_gain.astype(jnp.float32))
        .astype(jnp.bfloat16)
        .reshape(span_tokens, local_heads * head_width)
    )
    summed = summed_on_arrival(
        jnp.dot(head_out, out_weight, preferred_element_type=jnp.float32).astype(jnp.bfloat16),
        "tp",
        0,
    )
    return summed.astype(jnp.bfloat16)


def solution(mesh):
    finer = Mesh(mesh.devices.reshape(16, 4, 2, mesh.shape["tp"]), ("kv_0", "kv_1", "kv_2", "tp"))
    in_specs = (
        P(KV_TP, None),
        P(None, "tp"),
        P(),
        P("tp", None, None),
        P(),
        P(),
        P("tp", None, None),
        P("tp", None),
        P("tp", None),
        P(KV, None),
    )
    out_specs = P(KV_TP, None)
    return jax.shard_map(body, mesh=finer, in_specs=in_specs, out_specs=out_specs, check_vma=False)
```

profile of v0, /device:TPU:32, one launch (start us, length us, event | category | flops | bytes accessed | tf_op | source)
XLA Modules:
  0.0 241.8 jit_solution(4714949985406740218)
XLA Ops:
  6.5 0.7 all-gather.2.cloned.1.call-update
  7.3 0.7 broadcast_multiply_fusion
  8.3 3.7 %all_to_all.25 = s32[64,2,1]{0,2,1:T(1,128)S(1)} all-to-all(s32[64,2,1]{0,2,1:T(1,128)S(1)} %copy.25), channel_id=1, replica_groups=mesh['kv_0'=16,'kv_1'=4,'kv_2'=2,'tp'=4] {'kv_2'}, dimensions={1} | all-to-all | bytes 1024 | tf_op jit(solution)/shard_map/all_to_all | solution.py:29
  12.0 0.7 copy.26
  12.7 18.2 %all-to-all-start.1 = ((s32[64,2,1]{1,2,0:T(1,128)}), s32[64,2,1]{1,2,0:T(1,128)S(1)}, u32[]{:S(2)}, u32[]{:S(2)}) async-start(s32[64,2,1]{1,2,0:T(1,128)} %copy.26), calls=%async_computation.1 | async-start | bytes 65536 | tf_op jit(solution)/shard_map/all_to_all | solution.py:29
  30.9 0.7 convert_element_type.35
  31.6 13.0 %all-to-all-done.1 = s32[64,2,1]{1,2,0:T(1,128)S(1)} async-done(((s32[64,2,1]{1,2,0:T(1,128)}), s32[64,2,1]{1,2,0:T(1,128)S(1)}, u32[]{:S(2)}, u32[]{:S(2)}) %all-to-all-start.1) | async-done | bytes 544 | tf_op jit(solution)/shard_map/all_to_all | solution.py:29
  44.8 0.5 broadcast.155
  45.3 0.7 reduce.6
  46.2 5.9 %all-gather.2.cloned.1.call-done = bf16[512,2048]{1,0:T(8,128)(2,1)} async-done(((bf16[128,2048]{1,0:T(8,128)(2,1)}), bf16[512,2048]{1,0:T(8,128)(2,1)}) %all-gather.2.cloned.1.call-update) | async-done | bytes 2097168 | tf_op jit(solution)/shard_map/all_gather | solution.py:72
  52.0 2.6 %multiply_reduce_fusion.2 = (f32[512]{0:T(512)S(1)}, f32[512,256]{1,0:T(8,128)S(1)}) fusion(bf16[512,2048]{1,0:T(8,128)(2,1)} %all-gather.2.cloned.1.call-done, bf16[2048,256]{1,0:T(8,128)(2,1)} %param.12), kind=kOutput, calls=%fused_computation.31 | convolution fusion | flops 537132544 | bytes 3672064 | tf_op jit(solution)/shard_map/dot_general | solution.py:74
  54.9 0.6 gather_fusion
  55.5 0.2 broadcast_select_fusion
  55.7 71.5 %all_to_all.26 = bf16[128,16,256]{2,1,0:T(8,128)(2,1)S(1)} all-to-all(bf16[128,16,256]{2,1,0:T(8,128)(2,1)S(1)} %broadcast_select_fusion), channel_id=1, replica_groups=mesh['kv_0'=16,'kv_1'=4,'kv_2'=2,'tp'=4] {'kv_0','kv_1','kv_2'}, dimensions={0} | all-to-all | bytes 2097152 | tf_op jit(solution)/shard_map/all_to_all | solution.py:102
  127.2 2.3 broadcast_in_dim.77
  129.5 5.0 %all-to-all-start.3 = ((bf16[4,128,16,256]{3,2,1,0:T(8,128)(2,1)}), bf16[4,128,16,256]{3,2,1,0:T(8,128)(2,1)}, u32[]{:S(2)}, u32[]{:S(2)}) async-start(bf16[4,128,16,256]{3,2,1,0:T(8,128)(2,1)} %broadcast_in_dim.77), calls=%async_computation.3 | async-start | bytes 8388608 | tf_op jit(solution)/shard_map/all_to_all | solution.py:41
  135.2 0.4 broadcast_compare_fusion
  135.6 2.4 convolution_convert_fusion.1
  138.0 0.5 multiply_reduce_fusion
  138.4 0.2 multiply_convert_fusion
  138.7 45.6 %all-to-all-done.3 = bf16[4,128,16,256]{3,2,1,0:T(8,128)(2,1)} async-done(((bf16[4,128,16,256]{3,2,1,0:T(8,128)(2,1)}), bf16[4,128,16,256]{3,2,1,0:T(8,128)(2,1)}, u32[]{:S(2)}, u32[]{:S(2)}) %all-to-all-start.3) | async-done | bytes 4194336 | tf_op jit(solution)/shard_map/all_to_all | solution.py:41
  184.3 2.7 %copy.27 = bf16[4,128,16,256]{3,2,0,1:T(8,128)(2,1)S(1)} copy(bf16[4,128,16,256]{3,2,1,0:T(8,128)(2,1)} %all-to-all-done.3) | data formatting | bytes 8388608 | tf_op jit(solution)/shard_map/all_to_all | solution.py:41
  187.0 2.4 %pad_maximum_fusion = bf16[136,64,256]{2,1,0:T(8,128)(2,1)} fusion(bf16[128,64,256]{2,1,0:T(8,128)(2,1)S(1)} %bitcast.55, bf16[8,64,256]{2,1,0:T(8,128)(2,1)S(1)} %bitcast.61), kind=kLoop, calls=%fused_computation.3 | loop fusion | flops 2228224 | bytes 8912896 | tf_op jit(solution)/shard_map/concatenate | solution.py:104
  189.4 5.0 %gather_fusion.1 = bf16[128,64,256]{2,1,0:T(8,128)(2,1)} fusion(bf16[136,64,256]{2,1,0:T(8,128)(2,1)} %pad_maximum_fusion, s32[1024]{0:T(1024)S(1)} %pad_clamp_fusion), kind=kCustom, calls=%fused_computation.1 | custom fusion | bytes 8389120 | tf_op jit(solution)/shard_map/jit(_take)/gather | solution.py:106
  194.4 4.6 %bitcast_select_fusion.1 = bf16[8,1024,256]{2,1,0:T(8,128)(2,1)S(1)} fusion(pred[8,1024]{1,0:T(8,128)(4,1)S(1)} %broadcast_in_dim.71, bf16[8,1024,256]{2,1,0:T(8,128)(2,1)} %bitcast.54), kind=kLoop, calls=%fused_computation.9 | loop fusion | flops 2097152 | bytes 8396800 | tf_op jit(solution)/shard_map/jit(_take)/select_n | solution.py:106
  199.0 1.5 fusion.3
  200.5 2.2 fusion.22
  202.7 0.9 fusion.13
  203.6 0.3 multiply_reduce_fusion.1
  204.1 0.7 convolution_convert_fusion
  204.9 28.8 %all_to_all.27 = bf16[4,128,2048]{2,1,0:T(8,128)(2,1)S(1)} all-to-all(bf16[4,128,2048]{2,1,0:T(8,128)(2,1)S(1)} %bitcast.56), channel_id=1, replica_groups=mesh['kv_0'=16,'kv_1'=4,'kv_2'=2,'tp'=4] {'tp'}, dimensions={0} | all-to-all | bytes 4194304 | tf_op jit(solution)/shard_map/all_to_all | solution.py:51
  233.7 1.3 reduce_sum.52
  (44 shorter events, 1.6 us)
Async XLA Ops:
  6.5 197.6 %copy-start = (bf16[256,2048]{1,0:T(8,128)(2,1)S(1)}, bf16[256,2048]{1,0:T(8,128)(2,1)}, u32[]{:S(2)}) copy-start(bf16[256,2048]{1,0:T(8,128)(2,1)} %param.18) | copy-start | bytes 3145732
  6.5 45.5 %all-gather.2.cloned.1.call-start = ((), (), s32[]{:S(2)}) async-start(), calls=%async_computation.5 | async-start | bytes 2621440 | tf_op jit(solution)/shard_map/all_gather | solution.py:72
  12.7 31.9 %all-to-all-start.1 = ((s32[64,2,1]{1,2,0:T(1,128)}), s32[64,2,1]{1,2,0:T(1,128)S(1)}, u32[]{:S(2)}, u32[]{:S(2)}) async-start(s32[64,2,1]{1,2,0:T(1,128)} %copy.26), calls=%async_computation.1 | async-start | bytes 65536 | tf_op jit(solution)/shard_map/all_to_all | solution.py:29
  129.5 5.0 %copy-start.3 = (s32[8,16]{1,0:T(8,128)S(1)}, s32[8,16]{1,0:T(8,128)}, u32[]{:S(2)}) copy-start(s32[8,16]{1,0:T(8,128)} %param.19) | copy-start | bytes 1540
  129.5 5.3 %copy-start.5 = (bf16[256]{0:T(256)(128)(2,1)S(1)}, bf16[256]{0:T(256)(128)(2,1)}, u32[]{:S(2)}) copy-start(bf16[256]{0:T(256)(128)(2,1)} %param.14) | copy-start | bytes 1540
  129.5 5.6 %copy-start.6 = (bf16[2,128]{1,0:T(2,128)(2,1)S(1)}, bf16[2,128]{1,0:T(2,128)(2,1)}, u32[]{:S(2)}) copy-start(bf16[2,128]{1,0:T(2,128)(2,1)} %param.17) | copy-start | bytes 1540
  129.5 6.1 %copy-start.4 = (bf16[2048,256]{1,0:T(8,128)(2,1)S(1)}, bf16[2048,256]{1,0:T(8,128)(2,1)}, u32[]{:S(2)}) copy-start(bf16[2048,256]{1,0:T(8,128)(2,1)} %param.11) | copy-start | bytes 3145732
  129.5 54.8 %all-to-all-start.3 = ((bf16[4,128,16,256]{3,2,1,0:T(8,128)(2,1)}), bf16[4,128,16,256]{3,2,1,0:T(8,128)(2,1)}, u32[]{:S(2)}, u32[]{:S(2)}) async-start(bf16[4,128,16,256]{3,2,1,0:T(8,128)(2,1)} %broadcast_in_dim.77), calls=%async_computation.3 | async-start | bytes 8388608 | tf_op jit(solution)/shard_map/all_to_all | solution.py:41
  134.5 3.4 %copy-start.2 = (bf16[2,128,256]{2,1,0:T(8,128)(2,1)S(1)}, bf16[2,128,256]{2,1,0:T(8,128)(2,1)}, u32[]{:S(2)}) copy-start(bf16[2,128,256]{2,1,0:T(8,128)(2,1)} %param.13) | copy-start | bytes 393220
  202.7 1.0 copy-start.1
Sparse Core Ops, SparseCore 0:
  9.4 42.5 all-gather.1
where the time goes:
time: 242 us
  blocking collectives  104 us (43%)
  waiting for transfers between devices  65.2 us (27%)
  starting transfers between devices  23.2 us (10%)
  other arithmetic  13.9 us (6%)
  between operations  13.7 us (6%)
  local copies, waits for them, and re-layouts  13 us (5%)
  matrix products  8.93 us (4%)
    all_to_all x1, blocking collectives, body(): lax.all_to_all(outgoing, KV, split_axis=0, concat_axis=0, tiled=True)  71.5 us
    all_to_all x1, waiting for transfers between devices, copy_for_each(): return lax.all_to_all(copies, axis, split_axis=0, concat_axis=0, tiled=True)  45.6 us
    all_to_all x1, blocking collectives, summed_on_arrival(): lax.all_to_all(blocks, axis, split_axis=0, concat_axis=0, tiled=True)  28.8 us
    all_to_all x1, starting transfers between devices, moved_by_axis(): filled = lax.all_to_all(filled, axes[k], k, k, tiled=True)  18.2 us
    all_to_all x1, waiting for transfers between devices, moved_by_axis(): filled = lax.all_to_all(filled, axes[k], k, k, tiled=True)  13 us
    all_gather x1, waiting for transfers between devices, body(): shard_rows = lax.all_gather(tokens, 'tp', axis=0, tiled=True)  5.87 us
    gather x1, local copies, waits for them, and re-layouts, body(): jnp.take(key_table, table_slot, axis=0)  5.04 us
    all_to_all x1, starting transfers between devices, copy_for_each(): return lax.all_to_all(copies, axis, split_axis=0, concat_axis=0, tiled=True)  5 us
  transfers between devices with their start and end apart: 3, of which 3 were waited for; matrix products, arithmetic and copies ran while one was open for 3% of the time, Pallas kernels for 0%

commit v1 on v0

v1 whole, which is shorter than its diff:
```python
import functools

import jax
import jax.numpy as jnp
from jax import lax
from jax.experimental import pallas as pl
from jax.experimental.pallas import tpu as pltpu
from jax.sharding import Mesh
from jax.sharding import PartitionSpec as P

KV = ("kv_0", "kv_1", "kv_2")
KV_TP = ("kv_0", "kv_1", "kv_2", "tp")
MESH = pl.DeviceIdType.MESH
EPS = 1e-06
BF16 = jnp.bfloat16
F32 = jnp.float32
LOG2E = 1.4426950408889634


def rms(v, gain):
    return v * lax.rsqrt(jnp.mean(v * v, axis=-1, keepdims=True) + EPS) * gain


def kernel(
    dims,
    chosen,
    tokens_hbm,
    lw_hbm,
    qw_hbm,
    ka_hbm,
    va_hbm,
    ow_hbm,
    hg,
    qg,
    lg,
    out,
    *scratch,
):
    nz, nx, nc, ny, nsel, nloc = dims
    np_ = nx * nc
    sb = 2 * ny
    nr = nsel - nloc
    rsteps = nz // 2
    lsteps = nz - 1 - rsteps
    (
        tok, lw, wq, wo, ka, va, hgs, lat, span, piece0, want, wt, wts,
        xs, xr, ys, kvb, ab, kp, mix, ho,
        loc_sem, t_s, t_r, s_s, s_r, h_s, h_r, n_s, n_r, r_s, r_r, l_s, l_r,
        x_s, x_r, y_s, y_r, w1_s, w1_r, w2_s, w2_r, w3_s, w3_r,
        *ring,
    ) = scratch
    right = [piece0] + list(ring[:rsteps])
    left = [piece0] + list(ring[rsteps:])
    sh = piece0.shape[1]
    lat_w = piece0.shape[2]
    blk = sh * ny

    z = lax.axis_index("kv_0")
    x = lax.axis_index("kv_1")
    c = lax.axis_index("kv_2")
    y = lax.axis_index("tp")
    xc = x * nc + c

    def at_plane(d):
        p = lax.rem(xc + d + np_, np_)
        return {"kv_1": lax.div(p, nc), "kv_2": lax.rem(p, nc)}

    def at_y(e):
        return {"tp": lax.rem(y + e + ny, ny)}

    def at_z(d):
        return {"kv_0": lax.rem(z + d + nz, nz)}

    def at_x(d):
        return {"kv_1": lax.rem(x + d + nx, nx)}

    sent = []

    def send(src, dst, s, r, dev):
        cp = pltpu.make_async_remote_copy(
            src_ref=src, dst_ref=dst, send_sem=s, recv_sem=r,
            device_id=dev, device_id_type=MESH,
        )
        cp.start()
        sent.append(cp)

    def arrive(dst, s, r, dev):
        pltpu.make_async_remote_copy(
            src_ref=dst, dst_ref=dst, send_sem=s, recv_sem=r,
            device_id=dev, device_id_type=MESH,
        ).wait_recv()

    barrier = pltpu.get_barrier_semaphore()
    peers = [at_y(e) for e in range(1, ny)]
    peers += [at_z(1)] + ([at_z(-1)] if nz > 2 else [])
    peers += [at_plane(d) for d in range(1, np_)]
    for dev in peers:
        pl.semaphore_signal(barrier, inc=1, device_id=dev, device_id_type=MESH)

    tok_cp = pltpu.make_async_copy(tokens_hbm, tok, loc_sem.at[0])
    lw_cp = pltpu.make_async_copy(lw_hbm, lw, loc_sem.at[1])
    own_cps = [
        pltpu.make_async_copy(qw_hbm, wq.at[y], loc_sem.at[2]),
        pltpu.make_async_copy(ka_hbm, ka.at[y], loc_sem.at[3]),
        pltpu.make_async_copy(va_hbm, va.at[y], loc_sem.at[4]),
        pltpu.make_async_copy(ow_hbm, wo.at[y], loc_sem.at[5]),
    ]
    for cp in [tok_cp, lw_cp] + own_cps:
        cp.start()

    d_io = lax.broadcasted_iota(jnp.int32, (8, 128), 0)
    i_io = lax.broadcasted_iota(jnp.int32, (8, 128), 1)
    owner_of = lax.rem(z - lax.rem(i_io, nz) + nz, nz) * np_ + lax.rem(
        xc - lax.rem(d_io, np_) + np_, np_
    )
    acc = jnp.zeros((8, 128), jnp.int32)
    for row in range(sb):
        for p in range(nloc, nsel):
            v = chosen[row, p]
            acc = jnp.where(owner_of == lax.div(v, sb), lax.rem(v, sb), acc)
    for d in range(np_):
        row = jnp.broadcast_to(acc[d : d + 1], (8, 128))
        if d == 0:
            wt[0] = row
        else:
            want[d] = row

    tok_cp.wait()
    lw_cp.wait()
    values = jnp.dot(tok[...], lw[...], preferred_element_type=F32)
    latent = rms(values, lg[...].astype(F32)).astype(BF16).reshape(2, ny, sh, lat_w)
    lat[...] = latent
    span[pl.ds(2 * y, 2)] = latent
    piece0[pl.ds(2 * y, 2)] = lat[:, y]

    pl.semaphore_wait(barrier, len(peers))

    for e in range(1, ny):
        send(lat.at[:, lax.rem(y + e, ny)], piece0.at[pl.ds(2 * y, 2)], t_s.at[e], t_r.at[e], at_y(e))
    for d in range(1, np_):
        send(want.at[d], wt.at[d], n_s.at[d], n_r.at[d], at_plane(-d))
    for e in range(1, ny):
        send(lat, span.at[pl.ds(2 * y, 2)], s_s.at[e], s_r.at[e], at_y(e))
        send(hg, hgs.at[y], h_s.at[e], h_r.at[e], at_y(e))
    hgs[y] = hg[...]

    big = [(qw_hbm, wq), (ka_hbm, ka), (va_hbm, va), (ow_hbm, wo)]
    parts = 2 * nc
    px = lax.rem(x, 2)
    g_own = px * nc + c
    g_far = (1 - px) * nc + c
    g_mate = px * nc + (1 - c)
    g_far_mate = (1 - px) * nc + (1 - c)

    def rows_of(a, g, half=None):
        n = big[a][0].shape[0] // parts
        if half is None:
            return pl.ds(pl.multiple_of(g * n, n), n)
        return pl.ds(pl.multiple_of(g * n + half * (n // 2), n // 2), n // 2)

    order = [e for e in (1, ny - 1) if e >= 1] if ny > 2 else [1]
    order += [e for e in range(2, ny - 1)]
    for a in range(4):
        for e in order:
            send(
                big[a][0].at[rows_of(a, g_own)], big[a][1].at[y, rows_of(a, g_own)],
                w1_s.at[a, e], w1_r.at[a, e], at_y(e),
            )

    mate = {"kv_2": 1 - c}

    def spread(a):
        w = big[a][1]
        for e in order:
            ys_ = lax.rem(y - e + ny, ny)
            mine = w.at[ys_, rows_of(a, g_own)]
            arrive(mine, w1_s.at[a, e], w1_r.at[a, e], at_y(e))
            for half, dx in ((0, 1), (1, -1)):
                h = w.at[ys_, rows_of(a, g_own, half)]
                send(h, h, w2_s.at[a, e, half], w2_r.at[a, e, half], at_x(dx))
            if nc > 1:
                send(mine, mine, w3_s.at[a, e, 0], w3_r.at[a, e, 0], mate)

    def pass_on(a):
        w = big[a][1]
        for e in order:
            ys_ = lax.rem(y - e + ny, ny)
            for half in (0, 1):
                h = w.at[ys_, rows_of(a, g_far, half)]
                arrive(h, w2_s.at[a, e, half], w2_r.at[a, e, half], at_x(1))
            far = w.at[ys_, rows_of(a, g_far)]
            if nc > 1:
                send(far, far, w3_s.at[a, e, 1], w3_r.at[a, e, 1], mate)

    def collect(a):
        own_cps[a].wait()
        if nc > 1:
            w = big[a][1]
            for e in order:
                ys_ = lax.rem(y - e + ny, ny)
                for k, g in ((0, g_mate), (1, g_far_mate)):
                    arrive(w.at[ys_, rows_of(a, g)], w3_s.at[a, e, k], w3_r.at[a, e, k], mate)

    for e in range(1, ny):
        ys_ = lax.rem(y - e + ny, ny)
        arrive(piece0.at[pl.ds(2 * ys_, 2)], t_s.at[e], t_r.at[e], at_y(e))
    send(right[0], right[1], r_s.at[1], r_r.at[1], at_z(1))
    if lsteps:
        send(left[0], left[1], l_s.at[1], l_r.at[1], at_z(-1))
    for d in range(1, np_):
        arrive(wt.at[d], n_s.at[d], n_r.at[d], at_plane(d))
    wt_cp = pltpu.make_async_copy(wt, wts, loc_sem.at[6])
    wt_cp.start()
    wt_cp.wait()

    def select(ref, i):
        for d in range(np_):
            block = ref[wts[d, 0, i]]
            if d == 0:
                xr[i] = block
            else:
                xs[d * nz + i] = block

    groups = []

    def post(lo, n):
        k = len(groups)
        groups.append((lo, n))
        for d in range(1, np_):
            at = pl.ds(d * nz + lo, n)
            send(xs.at[at], xr.at[at], x_s.at[d, k], x_r.at[d, k], at_plane(d))

    select(piece0, 0)
    r_lo, l_hi = 0, nz
    for s in range(1, rsteps + 1):
        arrive(right[s], r_s.at[s], r_r.at[s], at_z(-1))
        if s < rsteps:
            send(right[s], right[s + 1], r_s.at[s + 1], r_r.at[s + 1], at_z(1))
        if s <= lsteps:
            arrive(left[s], l_s.at[s], l_r.at[s], at_z(1))
            if s < lsteps:
                send(left[s], left[s + 1], l_s.at[s + 1], l_r.at[s + 1], at_z(-1))
        select(right[s], s)
        if s <= lsteps:
            select(left[s], nz - s)
        if s % 2 == 0 or s >= rsteps - 1:
            post(r_lo, s + 1 - r_lo)
            r_lo = s + 1
            if s <= lsteps:
                post(nz - s, l_hi - (nz - s))
                l_hi = nz - s
        if s == max(1, rsteps - 2):
            spread(0)
            spread(1)
            spread(2)

    for k, (lo, n) in enumerate(groups):
        for d in range(1, np_):
            arrive(xr.at[pl.ds(d * nz + lo, n)], x_s.at[d, k], x_r.at[d, k], at_plane(d))

    for b in range(2):
        for e in list(range(1, ny)) + [0]:
            row = 2 * lax.rem(y + e, ny) + b
            for j in range(nr):
                o = lax.div(chosen[row, nloc + j], sb)
                i = lax.rem(z - lax.div(o, np_) + nz, nz)
                d = lax.rem(xc - lax.rem(o, np_) + np_, np_)
                block = xr[d * nz + i]
                if e == 0:
                    kvb[b, nloc + j, y] = block
                else:
                    ys[e - 1, b, j] = block
            if e:
                send(
                    ys.at[e - 1, b], kvb.at[b, pl.ds(nloc, nr), y],
                    y_s.at[e, b], y_r.at[e, b], at_y(e),
                )
    pass_on(0)
    pass_on(1)
    pass_on(2)
    spread(3)

    for e in range(1, ny):
        ys_ = lax.rem(y - e + ny, ny)
        arrive(span.at[pl.ds(2 * ys_, 2)], s_s.at[e], s_r.at[e], at_y(e))
        arrive(hgs.at[ys_], h_s.at[e], h_r.at[e], at_y(e))
    lane = lax.broadcasted_iota(jnp.int32, (8, 128), 1)
    first = ((z * nx + x) * nc + c) * sb
    for b in range(2):
        row = 2 * y + b
        for p in range(nloc):
            kvb[b, p] = span[lax.rem(chosen[row, p], sb)]
        for p in range(0, nsel, 2):
            base = jnp.where(lane < blk, chosen[row, p] * blk, chosen[row, p + 1] * blk - blk)
            kp[b, :, p * blk : (p + 2) * blk] = base + lane

    collect(0)
    collect(1)

    def project(g, _):
        q = jnp.dot(tok[...], wq[g], preferred_element_type=F32).astype(BF16)
        for hh in range(2):
            a = jnp.dot(q[:, hh * 128 : (hh + 1) * 128], ka[g, hh * 128 : (hh + 1) * 128, :], preferred_element_type=F32)
            a = rms(a, qg[...].astype(F32)).astype(BF16)
            at = pl.ds(pl.multiple_of((2 * g + hh) * blk, blk), blk)
            ab[0, at] = a[:blk]
            ab[1, at] = a[blk:]
        return 0

    lax.fori_loop(0, ny, project, 0)
    pass_on(3)
    collect(2)

    chunk = min(4, 2 * ny) * blk
    for b in range(2):
        for e in range(1, ny):
            ys_ = lax.rem(y - e + ny, ny)
            arrive(kvb.at[b, pl.ds(nloc, nr), ys_], y_s.at[e, b], y_r.at[e, b], at_y(e))
        keys = kvb[b].reshape(nsel * blk, lat_w)
        q_pos = (first + 2 * y + b) * blk + lax.rem(
            lax.broadcasted_iota(jnp.int32, (chunk, nsel * blk), 0), blk
        )
        seen = kp[b, 0:1, :] <= q_pos
        for i in range(2 * ny * blk // chunk):
            sc = lax.dot_general(
                ab[b, i * chunk : (i + 1) * chunk], keys, (((1,), (1,)), ((), ())),
                preferred_element_type=F32,
            )
            sc = jnp.where(seen, sc, -jnp.inf)
            top = jnp.max(sc, axis=-1, keepdims=True)
            ex = jnp.exp2((sc - top) * (LOG2E * lat_w ** (-0.5)))
            wgt = (ex * (1.0 / jnp.sum(ex, axis=-1, keepdims=True))).astype(BF16)
            mix[i * chunk : (i + 1) * chunk] = jnp.dot(
                wgt, keys, preferred_element_type=F32
            ).astype(BF16)
        for h in range(2 * ny):
            v = jnp.dot(
                mix[h * blk : (h + 1) * blk],
                va[h // 2, (h % 2) * lat_w : (h % 2 + 1) * lat_w, :],
                preferred_element_type=F32,
            )
            gain = hgs[h // 2, h % 2 : h % 2 + 1].astype(F32)
            ho[b * blk : (b + 1) * blk, h * 128 : (h + 1) * 128] = rms(v, gain).astype(BF16)

    collect(3)
    wide = min(512, out.shape[1])

    def finish(t, _):
        at = pl.ds(pl.multiple_of(t * wide, wide), wide)
        total = jnp.zeros((2 * blk, wide), F32)
        for g in range(ny):
            part = jnp.dot(ho[:, g * 256 : (g + 1) * 256], wo[g, :, at], preferred_element_type=F32)
            total = total + part.astype(BF16).astype(F32)
        out[:, at] = total.astype(BF16)
        return 0

    lax.fori_loop(0, out.shape[1] // wide, finish, 0)
    for cp in sent:
        cp.wait_send()


def body(dims, tokens, query_weight, latent_weight, key_absorb, query_gain, latent_gain, value_absorb, head_gain, out_weight, chosen):
    nz, nx, nc, ny, nsel, nloc = dims
    np_, sb, nr = nx * nc, 2 * ny, nsel - nloc
    rows, d = tokens.shape
    heads, hd, lat_w = key_absorb.shape
    blk = rows // 2
    sh = blk // ny
    any_ = pl.BlockSpec(memory_space=pl.ANY)
    vm = pl.BlockSpec(memory_space=pltpu.VMEM)
    dma = pltpu.SemaphoreType.DMA
    piece = pltpu.VMEM((sb, sh, lat_w), BF16)
    scratch = [
        pltpu.VMEM((rows, d), BF16),
        pltpu.VMEM((d, lat_w), BF16),
        pltpu.VMEM((ny, d, heads * hd), BF16),
        pltpu.VMEM((ny, heads * hd, d), BF16),
        pltpu.VMEM((ny, heads * hd, lat_w), BF16),
        pltpu.VMEM((ny, heads * lat_w, hd), BF16),
        pltpu.VMEM((ny, heads, hd), BF16),
        pltpu.VMEM((2, ny, sh, lat_w), BF16),
        pltpu.VMEM((sb, ny, sh, lat_w), BF16),
        piece,
        pltpu.VMEM((np_, 8, 128), jnp.int32),
        pltpu.VMEM((np_, 8, 128), jnp.int32),
        pltpu.SMEM((np_, 8, 128), jnp.int32),
        pltpu.VMEM((np_ * nz, sh, lat_w), BF16),
        pltpu.VMEM((np_ * nz, sh, lat_w), BF16),
        pltpu.VMEM((ny - 1, 2, nr, sh, lat_w), BF16),
        pltpu.VMEM((2, nsel, ny, sh, lat_w), BF16),
        pltpu.VMEM((2, 2 * ny * blk, lat_w), BF16),
        pltpu.VMEM((2, 8, nsel * blk), jnp.int32),
        pltpu.VMEM((2 * ny * blk, lat_w), BF16),
        pltpu.VMEM((rows, heads * ny * hd), BF16),
        dma((7,)),
        dma((ny,)), dma((ny,)), dma((ny,)), dma((ny,)), dma((ny,)), dma((ny,)),
        dma((np_,)), dma((np_,)),
        dma((nz,)), dma((nz,)), dma((nz,)), dma((nz,)),
        dma((np_, 10)), dma((np_, 10)),
        dma((ny, 2)), dma((ny, 2)),
        dma((4, ny)), dma((4, ny)),
        dma((4, ny, 2)), dma((4, ny, 2)),
        dma((4, ny, 2)), dma((4, ny, 2)),
    ] + [piece] * (nz - 1)
    return pl.pallas_call(
        functools.partial(kernel, dims),
        out_shape=jax.ShapeDtypeStruct((rows, d), BF16),
        in_specs=[pl.BlockSpec(memory_space=pltpu.SMEM)] + [any_] * 6 + [vm] * 3,
        out_specs=vm,
        scratch_shapes=scratch,
        compiler_params=pltpu.CompilerParams(
            collective_id=0, has_side_effects=True, vmem_limit_bytes=60 * 2**20
        ),
        name="attend",
    )(
        chosen,
        tokens,
        latent_weight,
        query_weight,
        key_absorb.reshape(heads * hd, lat_w),
        value_absorb.reshape(heads * lat_w, hd),
        out_weight,
        head_gain,
        query_gain.reshape(1, lat_w),
        latent_gain.reshape(1, lat_w),
    )


def build(devices, dims):
    nz, nx, nc, ny = dims[:4]
    finer = Mesh(devices.reshape(nz, nx, nc, ny), KV_TP)
    in_specs = (
        P(KV_TP, None),
        P(None, "tp"),
        P(),
        P("tp", None, None),
        P(),
        P(),
        P("tp", None, None),
        P("tp", None),
        P("tp", None),
        P(KV, None),
    )
    return jax.shard_map(
        functools.partial(body, dims), mesh=finer, in_specs=in_specs, out_specs=P(KV_TP, None), check_vma=False
    )


def solution(mesh):
    return build(mesh.devices, (16, 4, 2, mesh.shape["tp"], 16, 4))
```

time: 242 us -> 79.5 us (0.33)
  the two profiles are of different devices: /device:TPU:32 before, /device:TPU:1 now
where the time goes in v1:
time: 79.5 us; the launch traced here: 79.3 us
  Pallas kernels  75.5 us (95%)
  local copies, waits for them, and re-layouts  3.77 us (5%)
    pallas_call x1, Pallas kernels, body(): pl.pallas_call(functools.partial(kernel, dims), out_shape=jax.ShapeDtypeS...  75.5 us
    unnamed x5, local copies, waits for them, and re-layouts  2.63 us

profile of v1, /device:TPU:1, one launch (start us, length us, event | category | flops | bytes accessed | tf_op | source)
XLA Modules:
  0.0 79.3 jit_solution(1843590057615784609)
XLA Ops:
  0.0 0.0 copy-start
  0.0 0.7 copy-done
  0.7 0.0 copy-start.1
  0.7 0.6 reshape.14.qg
  1.2 0.1 copy-done.1
  1.3 0.6 reshape.15.lg
  1.9 75.5 %attend.1 = bf16[128,2048]{1,0:T(8,128)(2,1)} custom-call(s32[8,16]{1,0:T(8,128)} %chosen.1, bf16[128,2048]{1,0:T(8,128)(2,1)} %tokens_hbm.1, bf16[2048,256]{1,0:T(8,128)(2,1)} %lw_hbm.1, bf16[2048,256]{1,0:T(8,128)(2,1)} %qw_hbm.1, bf16[256,256]{1,0:T(8,128)(2,1)} %bitcast.2, bf16[512,128]{1,0:T(8,128)(2,1)} %bitcast.3, bf16[256,2048]{1,0:T(8,128)(2,1)} %ow_hbm.1, ...), custom_call_target="tpu_custom_call" | custom-call | tf_op jit(solution)/shard_map/attend/pallas_call | solution.py:405
  77.4 1.9 %copy.12 = bf16[128,2048]{1,0:T(8,128)(2,1)} copy(bf16[128,2048]{1,0:T(8,128)(2,1)} %attend.1) | data formatting | bytes 1048576
Async XLA Ops:
  0.0 0.7 copy-start
  0.7 0.7 copy-start.1

commit v2 on v1

v2 whole, which is shorter than its diff:
```python
import functools

import jax
import jax.numpy as jnp
from jax import lax
from jax.experimental import pallas as pl
from jax.experimental.pallas import tpu as pltpu
from jax.sharding import Mesh
from jax.sharding import PartitionSpec as P

KV = ("kv_0", "kv_1", "kv_2")
KV_TP = ("kv_0", "kv_1", "kv_2", "tp")
MESH = pl.DeviceIdType.MESH
EPS = 1e-06
BF16 = jnp.bfloat16
F32 = jnp.float32
LOG2E = 1.4426950408889634
CUTS = 4


def rms(v, gain):
    return v * lax.rsqrt(jnp.mean(v * v, axis=-1, keepdims=True) + EPS) * gain


def kernel(
    dims,
    chosen_hbm,
    tokens_hbm,
    lw_hbm,
    qw_hbm,
    ka_hbm,
    va_hbm,
    ow_hbm,
    hg,
    qg_hbm,
    lg_hbm,
    out,
    *scratch,
):
    nz, nx, nc, ny, nsel, nloc = dims
    np_ = nx * nc
    sb = 2 * ny
    nr = nsel - nloc
    rsteps = nz // 2
    lsteps = nz - 1 - rsteps
    (
        chosen, qg, lg, tok, lw, wq, wo, ka, va, hgs, lat, span, piece0, want, wt, wts,
        xs, xr, ys, kvb, ab, kp, mix, ho,
        loc_sem, small_s, small_r, r_s, r_r, l_s, l_r,
        x_s, x_r, y_s, y_r, w_s, w1_r, w2_r, w3_r,
        *ring,
    ) = scratch
    right = [piece0] + list(ring[:rsteps])
    left = [piece0] + list(ring[rsteps:])
    sh = piece0.shape[1]
    lat_w = piece0.shape[2]
    blk = sh * ny

    z = lax.axis_index("kv_0")
    x = lax.axis_index("kv_1")
    c = lax.axis_index("kv_2")
    y = lax.axis_index("tp")
    xc = x * nc + c

    def at_plane(d):
        p = lax.rem(xc + d + np_, np_)
        return {"kv_1": lax.div(p, nc), "kv_2": lax.rem(p, nc)}

    def at_y(e):
        return {"tp": lax.rem(y + e + ny, ny)}

    def at_z(d):
        return {"kv_0": lax.rem(z + d + nz, nz)}

    def at_x(d):
        return {"kv_1": lax.rem(x + d + nx, nx)}

    def when(cond, f):
        if cond is None:
            f()
        else:
            pl.when(cond)(f)

    def remote(src, dst, s, r, dev):
        return pltpu.make_async_remote_copy(
            src_ref=src, dst_ref=dst, send_sem=s, recv_sem=r,
            device_id=dev, device_id_type=MESH,
        )

    def send(src, dst, s, r, dev, cond=None):
        when(cond, remote(src, dst, s, r, dev).start)

    def arrive(ref, r, cond=None):
        when(cond, remote(ref, ref, loc_sem.at[0], r, at_y(1)).wait_recv)

    drains = []

    def drain(ref, s, cond=None):
        drains.append((cond, remote(ref, ref, s, loc_sem.at[0], at_y(1))))

    tok_cp = pltpu.make_async_copy(tokens_hbm, tok, loc_sem.at[0])
    lw_cp = pltpu.make_async_copy(lw_hbm, lw, loc_sem.at[1])
    own_cps = [
        pltpu.make_async_copy(qw_hbm, wq.at[y], loc_sem.at[2]),
        pltpu.make_async_copy(ka_hbm, ka.at[y], loc_sem.at[3]),
        pltpu.make_async_copy(va_hbm, va.at[y], loc_sem.at[4]),
        pltpu.make_async_copy(ow_hbm, wo.at[y], loc_sem.at[5]),
    ]
    small_cps = [
        pltpu.make_async_copy(chosen_hbm, chosen, loc_sem.at[7]),
        pltpu.make_async_copy(lg_hbm, lg, loc_sem.at[8]),
        pltpu.make_async_copy(qg_hbm, qg, loc_sem.at[9]),
        pltpu.make_async_copy(hg, hgs.at[y], loc_sem.at[10]),
    ]
    for cp in small_cps + [tok_cp, lw_cp] + own_cps:
        cp.start()

    xs[...] = jnp.zeros_like(xs)
    xr[...] = jnp.zeros_like(xr)

    barrier = pltpu.get_barrier_semaphore()
    peers = [at_y(e) for e in range(1, ny)]
    peers += [at_z(d) for d in sorted({1 % nz, 2 % nz, (nz - 1) % nz, (nz - 2) % nz} - {0})]
    peers += [at_plane(d) for d in range(1, np_)]
    for dev in peers:
        pl.semaphore_signal(barrier, inc=1, device_id=dev, device_id_type=MESH)

    d_io = lax.broadcasted_iota(jnp.int32, (8, 128), 0)
    i_io = lax.broadcasted_iota(jnp.int32, (8, 128), 1)
    owner_of = lax.rem(z - lax.rem(i_io, nz) + nz, nz) * np_ + lax.rem(
        xc - lax.rem(d_io, np_) + np_, np_
    )
    acc = jnp.zeros((8, 128), jnp.int32)
    small_cps[0].wait()
    for row in range(sb):
        for p in range(nloc, nsel):
            v = chosen[row, p]
            acc = jnp.where(owner_of == lax.div(v, sb), lax.rem(v, sb), acc)
    for d in range(np_):
        row = jnp.broadcast_to(acc[d : d + 1], (8, 128))
        if d == 0:
            wt[0] = row
        else:
            want[d] = row

    small_cps[1].wait()
    tok_cp.wait()
    lw_cp.wait()
    values = jnp.dot(tok[...], lw[...], preferred_element_type=F32)
    latent = rms(values, lg[...].astype(F32).reshape(1, lat_w)).astype(BF16).reshape(2, ny, sh, lat_w)
    lat[...] = latent
    span[pl.ds(2 * y, 2)] = latent
    piece0[pl.ds(2 * y, 2)] = lat[:, y]

    pl.semaphore_wait(barrier, len(peers))

    for e in range(1, ny):
        send(lat.at[:, lax.rem(y + e, ny)], piece0.at[pl.ds(2 * y, 2)], small_s.at[0], small_r.at[0], at_y(e))
    for d in range(1, np_):
        send(want.at[d], wt.at[d], small_s.at[1], small_r.at[1], at_plane(-d))
    others = piece0.at[pl.ds(0, 2 * (ny - 1))]
    drain(others, small_s.at[0])
    drain(wt.at[pl.ds(1, np_ - 1)], small_s.at[1])

    big = [(qw_hbm, wq), (ka_hbm, ka), (va_hbm, va), (ow_hbm, wo)]
    parts = 2 * nc
    near = [1, ny - 1] if ny > 2 else [1]
    nj = ny - 1
    shard_of = [lax.rem(y - e + ny, ny) for e in near]
    if ny > 2:
        shard_of.append(lax.rem(y + 2, ny))
    mate = {"kv_2": 1 - c}

    def rows_of(a, far=False, half=None):
        par = lax.rem(x if a < 3 else z, 2)
        g = (1 - par if far else par) * nc + c
        n = big[a][0].shape[0] // parts
        if half is None:
            return pl.ds(pl.multiple_of(g * n, n), n)
        return pl.ds(pl.multiple_of(g * n + half * (n // 2), n // 2), n // 2)

    def shares(a, k):
        n = big[a][0].shape[0] // parts
        return big[a][1].at[pl.ds(0, nj), pl.ds(0, k * n)]

    def launch(a):
        for j, e in enumerate(near):
            send(big[a][0].at[rows_of(a)], big[a][1].at[y, rows_of(a)], w_s.at[0, a], w1_r.at[a, j], at_y(e))
        drain(shares(a, 1), w_s.at[0, a])
        drain(shares(a, 1), w_s.at[1, a])
        if nc > 1:
            drain(shares(a, 2), w_s.at[2, a])

    def forward(a):
        w = big[a][1]
        for j in range(len(near)):
            arrive(w.at[shard_of[j], rows_of(a)], w1_r.at[a, j])
            if ny > 2:
                part = w.at[shard_of[j], rows_of(a, half=j)]
                send(part, part, w_s.at[0, a], w1_r.at[a, 2], at_y(near[j]))

    def spread(a, j):
        w = big[a][1]
        mine = w.at[shard_of[j], rows_of(a)]
        if j == 2:
            arrive(mine, w1_r.at[a, 2])
        for half, d in ((0, 1), (1, -1)):
            part = w.at[shard_of[j], rows_of(a, half=half)]
            send(part, part, w_s.at[1, a], w2_r.at[a, j], at_x(d) if a < 3 else at_z(d))
        if nc > 1:
            send(mine, mine, w_s.at[2, a], w3_r.at[a, 0], mate)

    def pass_on(a):
        w = big[a][1]
        for j in range(nj):
            far = w.at[shard_of[j], rows_of(a, far=True)]
            arrive(far, w2_r.at[a, j])
            if nc > 1:
                send(far, far, w_s.at[2, a], w3_r.at[a, 1], mate)

    def collect(a):
        own_cps[a].wait()
        if nc > 1:
            arrive(shares(a, 1), w3_r.at[a, 0])
            arrive(shares(a, 1), w3_r.at[a, 1])

    for a in range(3):
        launch(a)

    arrive(others, small_r.at[0])

    def targets(s, steps):
        ts = [1] if s < 2 else ([2, 1] if s % 2 == 0 else [])
        return [t for t in ts if s + t <= steps]

    cut = sb // CUTS
    r_hops = [(s, t) for s in range(rsteps) for t in targets(s, rsteps)]
    l_hops = [(s, t) for s in range(lsteps) for t in targets(s, lsteps)]

    def r_cond(s, t):
        return jnp.logical_and(z >= s, z + t <= nz - 1)

    def l_cond(s):
        return lax.rem(z + s, nz) < lsteps

    def hop_right(s, k):
        at = pl.ds(k * cut, cut)
        for t in targets(s, rsteps):
            h = r_hops.index((s, t))
            send(right[s].at[at], right[s + t].at[at], r_s.at[h], r_r.at[s + t - 1, k], at_z(t), r_cond(s, t))

    def hop_left(s, k):
        at = pl.ds(k * cut, cut)
        for t in targets(s, lsteps):
            h = l_hops.index((s, t))
            send(left[s].at[at], left[s + t].at[at], l_s.at[h], l_r.at[s + t - 1, k], at_z(-t), l_cond(s))

    for k in range(CUTS):
        hop_right(0, k)
        hop_left(0, k)
    for h, (s, t) in enumerate(r_hops):
        drain(right[s], r_s.at[h], r_cond(s, t))
    for h, (s, t) in enumerate(l_hops):
        drain(left[s], l_s.at[h], l_cond(s))

    for e in range(1, ny):
        send(lat, span.at[pl.ds(2 * y, 2)], small_s.at[2], small_r.at[2], at_y(e))
        send(hg, hgs.at[y], small_s.at[3], small_r.at[3], at_y(e))
    drain(span.at[pl.ds(0, 2 * (ny - 1))], small_s.at[2])
    drain(hgs.at[pl.ds(0, ny - 1)], small_s.at[3])

    arrive(wt.at[pl.ds(1, np_ - 1)], small_r.at[1])
    wt_cp = pltpu.make_async_copy(wt, wts, loc_sem.at[6])
    wt_cp.start()
    wt_cp.wait()

    def select(ref, i):
        for d in range(np_):
            block = ref[wts[d, 0, i]]
            if d == 0:
                xr[i] = block
            else:
                xs[d * nz + i] = block

    groups = []

    def post(lo, n, cond):
        k = len(groups)
        groups.append((n, cond))
        for d in range(1, np_):
            at = pl.ds(d * nz + lo, n)
            send(xs.at[at], xr.at[at], x_s.at[k], x_r.at[k], at_plane(d), cond)
        drain(xs.at[pl.ds(0, (np_ - 1) * n)], x_s.at[k], cond)

    def take(s):
        for k in range(CUTS):
            at = pl.ds(k * cut, cut)
            arrive(right[s].at[at], r_r.at[s - 1, k], z >= s)
            if s < rsteps:
                hop_right(s, k)
            if s <= lsteps:
                arrive(left[s].at[at], l_r.at[s - 1, k], l_cond(s))
                if s < lsteps:
                    hop_left(s, k)

    select(piece0, 0)
    r_lo, l_hi = 0, nz
    stages = [[1], [2]] + [[s + 1, s] for s in range(3, nz, 2)]
    for stage in stages:
        stage = [s for s in stage if s <= rsteps]
        if not stage:
            continue
        for s in stage:
            take(s)
        for s in stage:
            pl.when(z >= s)(functools.partial(select, right[s], s))
            if s <= lsteps:
                pl.when(z + s >= nz)(functools.partial(select, left[s], nz - s))
        top = max(stage)
        if top > 1 or top == rsteps:
            post(r_lo, top + 1 - r_lo, z >= r_lo)
            r_lo = top + 1
            l_top = min(top, lsteps)
            if nz - l_top < l_hi:
                post(nz - l_top, l_hi - (nz - l_top), z + l_top >= nz)
                l_hi = nz - l_top
        if 1 in stage:
            forward(0)
            for j in range(len(near)):
                spread(0, j)
        if 2 in stage or rsteps < 2:
            for a in (1, 2):
                forward(a)
                for j in range(len(near)):
                    spread(a, j)
            launch(3)
        if 4 in stage:
            for a in range(3):
                if nj > 2:
                    spread(a, 2)
        if 6 in stage:
            forward(3)
    if rsteps < 4 and nj > 2:
        for a in range(3):
            spread(a, 2)
    if rsteps < 6:
        forward(3)
    for j in range(len(near)):
        spread(3, j)
    for a in range(3):
        pass_on(a)
    if nj > 2:
        spread(3, 2)

    for k, (n, cond) in enumerate(groups):
        arrive(xr.at[pl.ds(0, (np_ - 1) * n)], x_r.at[k], cond)

    for b in range(2):
        for e in list(range(1, ny)) + [0]:
            row = 2 * lax.rem(y + e, ny) + b
            for j in range(nr):
                o = lax.div(chosen[row, nloc + j], sb)
                i = lax.rem(z - lax.div(o, np_) + nz, nz)
                d = lax.rem(xc - lax.rem(o, np_) + np_, np_)
                block = xr[d * nz + i]
                if e == 0:
                    kvb[b, nloc + j, y] = block
                else:
                    ys[e - 1, b, j] = block
            if e:
                send(ys.at[e - 1, b], kvb.at[b, pl.ds(nloc, nr), y], y_s.at[b], y_r.at[b], at_y(e))
        drain(ys.at[:, b], y_s.at[b])
    arrive(span.at[pl.ds(0, 2 * (ny - 1))], small_r.at[2])
    arrive(hgs.at[pl.ds(0, ny - 1)], small_r.at[3])
    lane = lax.broadcasted_iota(jnp.int32, (8, 128), 1)
    first = ((z * nx + x) * nc + c) * sb
    for b in range(2):
        row = 2 * y + b
        for p in range(nloc):
            kvb[b, p] = span[lax.rem(chosen[row, p], sb)]
        for p in range(0, nsel, 2):
            base = jnp.where(lane < blk, chosen[row, p] * blk, chosen[row, p + 1] * blk - blk)
            kp[b, :, p * blk : (p + 2) * blk] = base + lane

    small_cps[2].wait()
    small_cps[3].wait()
    collect(0)
    collect(1)

    def project(g, _):
        q = jnp.dot(tok[...], wq[g], preferred_element_type=F32).astype(BF16)
        for hh in range(2):
            a = jnp.dot(q[:, hh * 128 : (hh + 1) * 128], ka[g, hh * 128 : (hh + 1) * 128, :], preferred_element_type=F32)
            a = rms(a, qg[...].astype(F32).reshape(1, lat_w)).astype(BF16)
            at = pl.ds(pl.multiple_of((2 * g + hh) * blk, blk), blk)
            ab[0, at] = a[:blk]
            ab[1, at] = a[blk:]
        return 0

    lax.fori_loop(0, ny, project, 0)
    collect(2)

    chunk = min(4, 2 * ny) * blk
    for b in range(2):
        arrive(ys.at[:, b], y_r.at[b])
        keys = kvb[b].reshape(nsel * blk, lat_w)
        q_pos = (first + 2 * y + b) * blk + lax.rem(
            lax.broadcasted_iota(jnp.int32, (chunk, nsel * blk), 0), blk
        )
        seen = kp[b, 0:1, :] <= q_pos
        for i in range(2 * ny * blk // chunk):
            sc = lax.dot_general(
                ab[b, i * chunk : (i + 1) * chunk], keys, (((1,), (1,)), ((), ())),
                preferred_element_type=F32,
            )
            sc = jnp.where(seen, sc, -jnp.inf)
            top = jnp.max(sc, axis=-1, keepdims=True)
            ex = jnp.exp2((sc - top) * (LOG2E * lat_w ** (-0.5)))
            wgt = (ex * (1.0 / jnp.sum(ex, axis=-1, keepdims=True))).astype(BF16)
            mix[i * chunk : (i + 1) * chunk] = jnp.dot(
                wgt, keys, preferred_element_type=F32
            ).astype(BF16)
        for h in range(2 * ny):
            v = jnp.dot(
                mix[h * blk : (h + 1) * blk],
                va[h // 2, (h % 2) * lat_w : (h % 2 + 1) * lat_w, :],
                preferred_element_type=F32,
            )
            gain = hgs[h // 2, h % 2 : h % 2 + 1].astype(F32)
            ho[b * blk : (b + 1) * blk, h * 128 : (h + 1) * 128] = rms(v, gain).astype(BF16)
        if b == 0:
            pass_on(3)

    collect(3)
    wide = min(512, out.shape[1])

    def finish(t, _):
        at = pl.ds(pl.multiple_of(t * wide, wide), wide)
        total = jnp.zeros((2 * blk, wide), F32)
        for g in range(ny):
            part = jnp.dot(ho[:, g * 256 : (g + 1) * 256], wo[g, :, at], preferred_element_type=F32)
            total = total + part.astype(BF16).astype(F32)
        out[:, at] = total.astype(BF16)
        return 0

    lax.fori_loop(0, out.shape[1] // wide, finish, 0)
    for cond, cp in drains:
        when(cond, cp.wait_send)


def body(dims, tokens, query_weight, latent_weight, key_absorb, query_gain, latent_gain, value_absorb, head_gain, out_weight, chosen):
    nz, nx, nc, ny, nsel, nloc = dims
    np_, sb, nr = nx * nc, 2 * ny, nsel - nloc
    rows, d = tokens.shape
    heads, hd, lat_w = key_absorb.shape
    blk = rows // 2
    sh = blk // ny
    rsteps = nz // 2
    any_ = pl.BlockSpec(memory_space=pl.ANY)
    vm = pl.BlockSpec(memory_space=pltpu.VMEM)
    dma = pltpu.SemaphoreType.DMA
    piece = pltpu.VMEM((sb, sh, lat_w), BF16)
    scratch = [
        pltpu.SMEM((sb, nsel), jnp.int32),
        pltpu.VMEM((lat_w,), BF16),
        pltpu.VMEM((lat_w,), BF16),
        pltpu.VMEM((rows, d), BF16),
        pltpu.VMEM((d, lat_w), BF16),
        pltpu.VMEM((ny, d, heads * hd), BF16),
        pltpu.VMEM((ny, heads * hd, d), BF16),
        pltpu.VMEM((ny, heads * hd, lat_w), BF16),
        pltpu.VMEM((ny, heads * lat_w, hd), BF16),
        pltpu.VMEM((ny, heads, hd), BF16),
        pltpu.VMEM((2, ny, sh, lat_w), BF16),
        pltpu.VMEM((sb, ny, sh, lat_w), BF16),
        piece,
        pltpu.VMEM((np_, 8, 128), jnp.int32),
        pltpu.VMEM((np_, 8, 128), jnp.int32),
        pltpu.SMEM((np_, 8, 128), jnp.int32),
        pltpu.VMEM((np_ * nz, sh, lat_w), BF16),
        pltpu.VMEM((np_ * nz, sh, lat_w), BF16),
        pltpu.VMEM((ny - 1, 2, nr, sh, lat_w), BF16),
        pltpu.VMEM((2, nsel, ny, sh, lat_w), BF16),
        pltpu.VMEM((2, 2 * ny * blk, lat_w), BF16),
        pltpu.VMEM((2, 8, nsel * blk), jnp.int32),
        pltpu.VMEM((2 * ny * blk, lat_w), BF16),
        pltpu.VMEM((rows, heads * ny * hd), BF16),
        dma((11,)),
        dma((4,)), dma((4,)),
        dma((rsteps + 4,)), dma((rsteps, CUTS)), dma((rsteps + 4,)), dma((rsteps, CUTS)),
        dma((10,)), dma((10,)),
        dma((2,)), dma((2,)),
        dma((3, 4)), dma((4, 3)), dma((4, 3)), dma((4, 2)),
    ] + [piece] * (nz - 1)
    return pl.pallas_call(
        functools.partial(kernel, dims),
        out_shape=jax.ShapeDtypeStruct((rows, d), BF16),
        in_specs=[any_] * 10,
        out_specs=vm,
        scratch_shapes=scratch,
        compiler_params=pltpu.CompilerParams(
            collective_id=0, has_side_effects=True, vmem_limit_bytes=60 * 2**20
        ),
        name="attend",
    )(
        chosen,
        tokens,
        latent_weight,
        query_weight,
        key_absorb.reshape(heads * hd, lat_w),
        value_absorb.reshape(heads * lat_w, hd),
        out_weight,
        head_gain,
        query_gain,
        latent_gain,
    )


def build(devices, dims):
    nz, nx, nc, ny = dims[:4]
    finer = Mesh(devices.reshape(nz, nx, nc, ny), KV_TP)
    in_specs = (
        P(KV_TP, None),
        P(None, "tp"),
        P(),
        P("tp", None, None),
        P(),
        P(),
        P("tp", None, None),
        P("tp", None),
        P("tp", None),
        P(KV, None),
    )
    return jax.shard_map(
        functools.partial(body, dims), mesh=finer, in_specs=in_specs, out_specs=P(KV_TP, None), check_vma=False
    )


def solution(mesh):
    return build(mesh.devices, (16, 4, 2, mesh.shape["tp"], 16, 4))
```

time: 79.5 us -> 56.2 us (0.71)
  Pallas kernels: 75.5 us -> 54.2 us
  local copies, waits for them, and re-layouts: 3.77 us -> 1.88 us
    pallas_call x1, Pallas kernels: 75.5 us -> 54.2 us  [body(): pl.pallas_call(functools.partial(kernel, dims), out_shape=jax.ShapeDtypeS...]
    reshape x2 -> x0, local copies, waits for them, and re-layouts: 1.15 us -> none  [the longest x1 0.58 us: body(): latent_gain.reshape(1, lat_w)]
    unnamed x5 -> x1, local copies, waits for them, and re-layouts: 2.63 us -> 1.88 us
where the time goes in v2:
time: 56.2 us; the launch traced here: 56 us
  Pallas kernels  54.2 us (96%)
  local copies, waits for them, and re-layouts  1.88 us (3%)
    pallas_call x1, Pallas kernels, body(): pl.pallas_call(functools.partial(kernel, dims), out_shape=jax.ShapeDtypeS...  54.2 us
    unnamed x1, local copies, waits for them, and re-layouts  1.88 us

profile of v2, /device:TPU:1, one launch (start us, length us, event | category | flops | bytes accessed | tf_op | source)
XLA Modules:
  0.0 56.0 jit_solution(680754328220721154)
XLA Ops:
  0.0 54.2 %attend.1 = bf16[128,2048]{1,0:T(8,128)(2,1)} custom-call(s32[8,16]{1,0:T(8,128)} %chosen_hbm.1, bf16[128,2048]{1,0:T(8,128)(2,1)} %tokens_hbm.1, bf16[2048,256]{1,0:T(8,128)(2,1)} %lw_hbm.1, bf16[2048,256]{1,0:T(8,128)(2,1)} %qw_hbm.1, bf16[256,256]{1,0:T(8,128)(2,1)} %bitcast.2, bf16[512,128]{1,0:T(8,128)(2,1)} %bitcast.3, bf16[256,2048]{1,0:T(8,128)(2,1)} %ow_hbm.1, ...), custom_call_target="tpu_custom_call" | custom-call | tf_op jit(solution)/shard_map/attend/pallas_call | solution.py:495
  54.2 1.9 %copy.12 = bf16[128,2048]{1,0:T(8,128)(2,1)} copy(bf16[128,2048]{1,0:T(8,128)(2,1)} %attend.1) | data formatting | bytes 1048576

commit v3 on v2

--- a/solution.py
+++ b/solution.py
@@ -47,7 +47,7 @@
         chosen, qg, lg, tok, lw, wq, wo, ka, va, hgs, lat, span, piece0, want, wt, wts,
         xs, xr, ys, kvb, ab, kp, mix, ho,
         loc_sem, small_s, small_r, r_s, r_r, l_s, l_r,
-        x_s, x_r, y_s, y_r, w_s, w1_r, w2_r, w3_r,
+        x_s, x_r, y_s, y_r, w_s, w1_r, w2_r, w3_r, res, out_sem, ready,
         *ring,
     ) = scratch
     right = [piece0] + list(ring[:rsteps])
@@ -93,10 +93,42 @@
     def arrive(ref, r, cond=None):
         when(cond, remote(ref, ref, loc_sem.at[0], r, at_y(1)).wait_recv)
 
-    drains = []
-
-    def drain(ref, s, cond=None):
-        drains.append((cond, remote(ref, ref, s, loc_sem.at[0], at_y(1))))
+    drains, late = [], []
+
+    def drain(ref, s, cond=None, to=drains):
+        to.append((cond, remote(ref, ref, s, loc_sem.at[0], at_y(1))))
+
+    def flush(queue):
+        for cond, cp in queue:
+            when(cond, cp.wait_send)
+        queue.clear()
+
+    split = nz > 4
+    offsets = sorted({1 % nz, 2 % nz, (nz - 1) % nz, (nz - 2) % nz} - {0})
+    barrier = pltpu.get_barrier_semaphore()
+    peers = [(at_y(e), None) for e in range(1, ny)]
+    peers += [(at_z(d), z + d < nz if split and d < 3 else None) for d in offsets]
+    peers += [(at_plane(d), None) for d in range(1, np_)]
+
+    def greet(sem, dev):
+        pl.semaphore_signal(sem, inc=1, device_id=dev, device_id_type=MESH)
+
+    for dev, cond in peers:
+        when(cond, functools.partial(greet, barrier, dev))
+
+    def enter():
+        if not split:
+            pl.semaphore_wait(barrier, len(peers))
+            return
+        for k, cond in ((0, z >= 2), (1, z == 1), (2, z == 0)):
+            pl.when(cond)(functools.partial(pl.semaphore_wait, barrier, len(peers) - k))
+        for d in (1, 2):
+            pl.when(z + d >= nz)(functools.partial(greet, ready, at_z(d)))
+
+    def wait_wrap():
+        if split:
+            pl.when(z == 0)(functools.partial(pl.semaphore_wait, ready, 2))
+            pl.when(z == 1)(functools.partial(pl.semaphore_wait, ready, 1))
 
     tok_cp = pltpu.make_async_copy(tokens_hbm, tok, loc_sem.at[0])
     lw_cp = pltpu.make_async_copy(lw_hbm, lw, loc_sem.at[1])
@@ -117,13 +149,6 @@
 
     xs[...] = jnp.zeros_like(xs)
     xr[...] = jnp.zeros_like(xr)
-
-    barrier = pltpu.get_barrier_semaphore()
-    peers = [at_y(e) for e in range(1, ny)]
-    peers += [at_z(d) for d in sorted({1 % nz, 2 % nz, (nz - 1) % nz, (nz - 2) % nz} - {0})]
-    peers += [at_plane(d) for d in range(1, np_)]
-    for dev in peers:
-        pl.semaphore_signal(barrier, inc=1, device_id=dev, device_id_type=MESH)
 
     d_io = lax.broadcasted_iota(jnp.int32, (8, 128), 0)
     i_io = lax.broadcasted_iota(jnp.int32, (8, 128), 1)
@@ -152,7 +177,7 @@
     span[pl.ds(2 * y, 2)] = latent
     piece0[pl.ds(2 * y, 2)] = lat[:, y]
 
-    pl.semaphore_wait(barrier, len(peers))
+    enter()
 
     for e in range(1, ny):
         send(lat.at[:, lax.rem(y + e, ny)], piece0.at[pl.ds(2 * y, 2)], small_s.at[0], small_r.at[0], at_y(e))
@@ -186,10 +211,17 @@
     def launch(a):
         for j, e in enumerate(near):
             send(big[a][0].at[rows_of(a)], big[a][1].at[y, rows_of(a)], w_s.at[0, a], w1_r.at[a, j], at_y(e))
-        drain(shares(a, 1), w_s.at[0, a])
-        drain(shares(a, 1), w_s.at[1, a])
+        drain(shares(a, 1), w_s.at[0, a], to=late)
+        if a < 3:
+            drain(shares(a, 1), w_s.at[1, a], to=late)
+        else:
+            n = big[a][0].shape[0] // parts // 2
+            halves = big[a][1].at[pl.ds(0, nj), pl.ds(0, n)]
+            drain(halves, w_s.at[1, a], to=late)
+            drain(halves, w_s.at[3, a], z < nz - 1, to=late)
+            drain(halves, w_s.at[4, a], z == 1, to=late)
         if nc > 1:
-            drain(shares(a, 2), w_s.at[2, a])
+            drain(shares(a, 2), w_s.at[2, a], to=late)
 
     def forward(a):
         w = big[a][1]
@@ -204,25 +236,28 @@
         mine = w.at[shard_of[j], rows_of(a)]
         if j == 2:
             arrive(mine, w1_r.at[a, 2])
-        for half, d in ((0, 1), (1, -1)):
-            part = w.at[shard_of[j], rows_of(a, half=half)]
-            send(part, part, w_s.at[1, a], w2_r.at[a, j], at_x(d) if a < 3 else at_z(d))
+        lo, hi = (w.at[shard_of[j], rows_of(a, half=half)] for half in (0, 1))
+        if a < 3:
+            send(lo, lo, w_s.at[1, a], w2_r.at[a, j], at_x(1))
+            send(hi, hi, w_s.at[1, a], w2_r.at[a, j], at_x(-1))
+        else:
+            send(hi, hi, w_s.at[1, a], w2_r.at[a, j], at_z(-1))
+            send(lo, lo, w_s.at[3, a], w2_r.at[a, j], at_z(1), z < nz - 1)
+            send(lo, lo, w_s.at[4, a], w2_r.at[a, j], at_z(-1), z == 1)
         if nc > 1:
-            send(mine, mine, w_s.at[2, a], w3_r.at[a, 0], mate)
-
-    def pass_on(a):
-        w = big[a][1]
-        for j in range(nj):
-            far = w.at[shard_of[j], rows_of(a, far=True)]
-            arrive(far, w2_r.at[a, j])
-            if nc > 1:
-                send(far, far, w_s.at[2, a], w3_r.at[a, 1], mate)
-
-    def collect(a):
-        own_cps[a].wait()
+            send(mine, mine, w_s.at[2, a], w3_r.at[a, j, 0], mate)
+
+    def pass_on(a, j):
+        far = big[a][1].at[shard_of[j], rows_of(a, far=True)]
+        arrive(far, w2_r.at[a, j])
         if nc > 1:
-            arrive(shares(a, 1), w3_r.at[a, 0])
-            arrive(shares(a, 1), w3_r.at[a, 1])
+            send(far, far, w_s.at[2, a], w3_r.at[a, j, 1], mate)
+
+    def collect(a, j):
+        if nc > 1:
+            slice_ = big[a][1].at[0, pl.ds(0, big[a][0].shape[0] // parts)]
+            arrive(slice_, w3_r.at[a, j, 0])
+            arrive(slice_, w3_r.at[a, j, 1])
 
     for a in range(3):
         launch(a)
@@ -249,25 +284,20 @@
             h = r_hops.index((s, t))
             send(right[s].at[at], right[s + t].at[at], r_s.at[h], r_r.at[s + t - 1, k], at_z(t), r_cond(s, t))
 
-    def hop_left(s, k):
+    def hop_left(s, k, cond=None):
         at = pl.ds(k * cut, cut)
         for t in targets(s, lsteps):
             h = l_hops.index((s, t))
-            send(left[s].at[at], left[s + t].at[at], l_s.at[h], l_r.at[s + t - 1, k], at_z(-t), l_cond(s))
+            ok = l_cond(s) if cond is None else cond
+            send(left[s].at[at], left[s + t].at[at], l_s.at[h], l_r.at[s + t - 1, k], at_z(-t), ok)
 
     for k in range(CUTS):
         hop_right(0, k)
-        hop_left(0, k)
+        hop_left(0, k, jnp.logical_and(l_cond(0), z > 0) if split else None)
     for h, (s, t) in enumerate(r_hops):
         drain(right[s], r_s.at[h], r_cond(s, t))
     for h, (s, t) in enumerate(l_hops):
         drain(left[s], l_s.at[h], l_cond(s))
-
-    for e in range(1, ny):
-        send(lat, span.at[pl.ds(2 * y, 2)], small_s.at[2], small_r.at[2], at_y(e))
-        send(hg, hgs.at[y], small_s.at[3], small_r.at[3], at_y(e))
-    drain(span.at[pl.ds(0, 2 * (ny - 1))], small_s.at[2])
-    drain(hgs.at[pl.ds(0, ny - 1)], small_s.at[3])
 
     arrive(wt.at[pl.ds(1, np_ - 1)], small_r.at[1])
     wt_cp = pltpu.make_async_copy(wt, wts, loc_sem.at[6])
@@ -303,7 +333,29 @@
                 if s < lsteps:
                     hop_left(s, k)
 
+    early = z < nz // 2
+    first_two = z < min(2, nz // 2)
+    middle = jnp.logical_and(early, z >= 2)
+
+    def spread_out():
+        for j in range(len(near)):
+            spread(3, j)
+
+    def spread_two():
+        for a in range(3):
+            spread(a, 2)
+
+    def first_planes():
+        if nj > 2:
+            spread_two()
+        forward(3)
+        spread_out()
+
     select(piece0, 0)
+    wait_wrap()
+    if split:
+        for k in range(CUTS):
+            hop_left(0, k, z == 0)
     r_lo, l_hi = 0, nz
     stages = [[1], [2]] + [[s + 1, s] for s in range(3, nz, 2)]
     for stage in stages:
@@ -335,25 +387,37 @@
                     spread(a, j)
             launch(3)
         if 4 in stage:
-            for a in range(3):
-                if nj > 2:
-                    spread(a, 2)
+            pl.when(first_two)(first_planes)
+            if nj > 2:
+                pl.when(middle)(spread_two)
         if 6 in stage:
-            forward(3)
-    if rsteps < 4 and nj > 2:
-        for a in range(3):
-            spread(a, 2)
+            pl.when(jnp.logical_not(first_two))(functools.partial(forward, 3))
+            pl.when(middle)(spread_out)
+    if rsteps < 4:
+        pl.when(first_two)(first_planes)
+        if nj > 2:
+            pl.when(middle)(spread_two)
     if rsteps < 6:
-        forward(3)
-    for j in range(len(near)):
-        spread(3, j)
+        pl.when(jnp.logical_not(first_two))(functools.partial(forward, 3))
+        pl.when(middle)(spread_out)
+    for e in range(1, ny):
+        send(lat, span.at[pl.ds(2 * y, 2)], small_s.at[2], small_r.at[2], at_y(e))
+        send(hg, hgs.at[y], small_s.at[3], small_r.at[3], at_y(e))
+    drain(span.at[pl.ds(0, 2 * (ny - 1))], small_s.at[2])
+    drain(hgs.at[pl.ds(0, ny - 1)], small_s.at[3])
+
+    pl.when(jnp.logical_not(early))(spread_out)
     for a in range(3):
-        pass_on(a)
+        for j in range(len(near)):
+            pass_on(a, j)
     if nj > 2:
         spread(3, 2)
 
     for k, (n, cond) in enumerate(groups):
         arrive(xr.at[pl.ds(0, (np_ - 1) * n)], x_r.at[k], cond)
+
+    if nj > 2:
+        pl.when(jnp.logical_not(early))(spread_two)
 
     for b in range(2):
         for e in list(range(1, ny)) + [0]:
@@ -369,7 +433,7 @@
                     ys[e - 1, b, j] = block
             if e:
                 send(ys.at[e - 1, b], kvb.at[b, pl.ds(nloc, nr), y], y_s.at[b], y_r.at[b], at_y(e))
-        drain(ys.at[:, b], y_s.at[b])
+        drain(ys.at[:, b], y_s.at[b], to=late)
     arrive(span.at[pl.ds(0, 2 * (ny - 1))], small_r.at[2])
     arrive(hgs.at[pl.ds(0, ny - 1)], small_r.at[3])
     lane = lax.broadcasted_iota(jnp.int32, (8, 128), 1)
@@ -384,10 +448,13 @@
 
     small_cps[2].wait()
     small_cps[3].wait()
-    collect(0)
-    collect(1)
-
-    def project(g, _):
+    for cp in own_cps[:3]:
+        cp.wait()
+    for j in range(len(near)):
+        for a in range(3):
+            collect(a, j)
+
+    def project(g):
         q = jnp.dot(tok[...], wq[g], preferred_element_type=F32).astype(BF16)
         for hh in range(2):
             a = jnp.dot(q[:, hh * 128 : (hh + 1) * 128], ka[g, hh * 128 : (hh + 1) * 128, :], preferred_element_type=F32)
@@ -395,10 +462,19 @@
             at = pl.ds(pl.multiple_of((2 * g + hh) * blk, blk), blk)
             ab[0, at] = a[:blk]
             ab[1, at] = a[blk:]
+
+    def project_near(i, _):
+        project(lax.rem(y + ny + lax.rem(i + 1, 3) - 1, ny))
         return 0
 
-    lax.fori_loop(0, ny, project, 0)
-    collect(2)
+    lax.fori_loop(0, len(near) + 1, project_near, 0)
+    flush(drains)
+    if nj > 2:
+        for a in range(3):
+            pass_on(a, 2)
+        for a in range(3):
+            collect(a, 2)
+        project(shard_of[2])
 
     chunk = min(4, 2 * ny) * blk
     for b in range(2):
@@ -429,10 +505,18 @@
             gain = hgs[h // 2, h % 2 : h % 2 + 1].astype(F32)
             ho[b * blk : (b + 1) * blk, h * 128 : (h + 1) * 128] = rms(v, gain).astype(BF16)
         if b == 0:
-            pass_on(3)
-
-    collect(3)
+            for j in range(nj):
+                pass_on(3, j)
+
+    own_cps[3].wait()
+    for j in range(nj):
+        collect(3, j)
     wide = min(512, out.shape[1])
+    tiles = out.shape[1] // wide
+
+    def out_cp(t):
+        at = pl.ds(pl.multiple_of(t * wide, wide), wide)
+        return pltpu.make_async_copy(res.at[:, at], out.at[:, at], out_sem.at[t])
 
     def finish(t, _):
         at = pl.ds(pl.multiple_of(t * wide, wide), wide)
@@ -440,12 +524,14 @@
         for g in range(ny):
             part = jnp.dot(ho[:, g * 256 : (g + 1) * 256], wo[g, :, at], preferred_element_type=F32)
             total = total + part.astype(BF16).astype(F32)
-        out[:, at] = total.astype(BF16)
+        res[:, at] = total.astype(BF16)
+        out_cp(t).start()
         return 0
 
-    lax.fori_loop(0, out.shape[1] // wide, finish, 0)
-    for cond, cp in drains:
-        when(cond, cp.wait_send)
+    lax.fori_loop(0, tiles, finish, 0)
+    flush(late)
+    for t in range(tiles):
+        out_cp(t).wait()
 
 
 def body(dims, tokens, query_weight, latent_weight, key_absorb, query_gain, latent_gain, value_absorb, head_gain, out_weight, chosen):
@@ -457,7 +543,6 @@
     sh = blk // ny
     rsteps = nz // 2
     any_ = pl.BlockSpec(memory_space=pl.ANY)
-    vm = pl.BlockSpec(memory_space=pltpu.VMEM)
     dma = pltpu.SemaphoreType.DMA
     piece = pltpu.VMEM((sb, sh, lat_w), BF16)
     scratch = [
@@ -490,13 +575,14 @@
         dma((rsteps + 4,)), dma((rsteps, CUTS)), dma((rsteps + 4,)), dma((rsteps, CUTS)),
         dma((10,)), dma((10,)),
         dma((2,)), dma((2,)),
-        dma((3, 4)), dma((4, 3)), dma((4, 3)), dma((4, 2)),
+        dma((5, 4)), dma((4, 3)), dma((4, 3)), dma((4, 3, 2)),
+        pltpu.VMEM((rows, d), BF16), dma((4,)), pltpu.SemaphoreType.REGULAR,
     ] + [piece] * (nz - 1)
     return pl.pallas_call(
         functools.partial(kernel, dims),
         out_shape=jax.ShapeDtypeStruct((rows, d), BF16),
         in_specs=[any_] * 10,
-        out_specs=vm,
+        out_specs=any_,
         scratch_shapes=scratch,
         compiler_params=pltpu.CompilerParams(
             collective_id=0, has_side_effects=True, vmem_limit_bytes=60 * 2**20

time: 56.2 us -> 53.9 us (0.959)
  Pallas kernels: 54.2 us -> 51.9 us
    pallas_call x1, Pallas kernels: 54.2 us -> 51.9 us  [body(): pl.pallas_call(functools.partial(kernel, dims), out_shape=jax.ShapeDtypeS...]
where the time goes in v3:
time: 53.9 us; the launch traced here: 53.8 us
  Pallas kernels  51.9 us (96%)
  local copies, waits for them, and re-layouts  1.88 us (3%)
    pallas_call x1, Pallas kernels, body(): pl.pallas_call(functools.partial(kernel, dims), out_shape=jax.ShapeDtypeS...  51.9 us
    unnamed x1, local copies, waits for them, and re-layouts  1.88 us

profile of v3, /device:TPU:1, one launch (start us, length us, event | category | flops | bytes accessed | tf_op | source)
XLA Modules:
  0.0 53.8 jit_solution(9325705946966240186)
XLA Ops:
  0.0 51.9 %attend.1 = bf16[128,2048]{1,0:T(8,128)(2,1)} custom-call(s32[8,16]{1,0:T(8,128)} %chosen_hbm.1, bf16[128,2048]{1,0:T(8,128)(2,1)} %tokens_hbm.1, bf16[2048,256]{1,0:T(8,128)(2,1)} %lw_hbm.1, bf16[2048,256]{1,0:T(8,128)(2,1)} %qw_hbm.1, bf16[256,256]{1,0:T(8,128)(2,1)} %bitcast.2, bf16[512,128]{1,0:T(8,128)(2,1)} %bitcast.3, bf16[256,2048]{1,0:T(8,128)(2,1)} %ow_hbm.1, ...), custom_call_target="tpu_custom_call" | custom-call | tf_op jit(solution)/shard_map/attend/pallas_call | solution.py:581
  51.9 1.9 %copy.12 = bf16[128,2048]{1,0:T(8,128)(2,1)} copy(bf16[128,2048]{1,0:T(8,128)(2,1)} %attend.1) | data formatting | bytes 1048576

commit v4 on v3

--- a/solution.py
+++ b/solution.py
@@ -144,7 +144,7 @@
         pltpu.make_async_copy(qg_hbm, qg, loc_sem.at[9]),
         pltpu.make_async_copy(hg, hgs.at[y], loc_sem.at[10]),
     ]
-    for cp in small_cps + [tok_cp, lw_cp] + own_cps:
+    for cp in small_cps + [tok_cp, lw_cp]:
         cp.start()
 
     xs[...] = jnp.zeros_like(xs)
@@ -171,15 +171,19 @@
     small_cps[1].wait()
     tok_cp.wait()
     lw_cp.wait()
+    for cp in own_cps:
+        cp.start()
     values = jnp.dot(tok[...], lw[...], preferred_element_type=F32)
     latent = rms(values, lg[...].astype(F32).reshape(1, lat_w)).astype(BF16).reshape(2, ny, sh, lat_w)
     lat[...] = latent
     span[pl.ds(2 * y, 2)] = latent
     piece0[pl.ds(2 * y, 2)] = lat[:, y]
 
+    far_y = sorted(range(1, ny), key=lambda e: -min(e, ny - e))
+    far_x = sorted(range(1, np_), key=lambda d: -min(d, np_ - d))
     enter()
 
-    for e in range(1, ny):
+    for e in far_y:
         send(lat.at[:, lax.rem(y + e, ny)], piece0.at[pl.ds(2 * y, 2)], small_s.at[0], small_r.at[0], at_y(e))
     for d in range(1, np_):
         send(want.at[d], wt.at[d], small_s.at[1], small_r.at[1], at_plane(-d))
@@ -317,7 +321,7 @@
     def post(lo, n, cond):
         k = len(groups)
         groups.append((n, cond))
-        for d in range(1, np_):
+        for d in far_x:
             at = pl.ds(d * nz + lo, n)
             send(xs.at[at], xr.at[at], x_s.at[k], x_r.at[k], at_plane(d), cond)
         drain(xs.at[pl.ds(0, (np_ - 1) * n)], x_s.at[k], cond)
@@ -351,7 +355,17 @@
         forward(3)
         spread_out()
 
+    def first_weights():
+        forward(0)
+        for j in range(len(near)):
+            spread(0, j)
+
+    def pass_out():
+        for j in range(len(near)):
+            pass_on(3, j)
+
     select(piece0, 0)
+    pl.when(first_two)(first_weights)
     wait_wrap()
     if split:
         for k in range(CUTS):
@@ -377,9 +391,7 @@
                 post(nz - l_top, l_hi - (nz - l_top), z + l_top >= nz)
                 l_hi = nz - l_top
         if 1 in stage:
-            forward(0)
-            for j in range(len(near)):
-                spread(0, j)
+            pl.when(jnp.logical_not(first_two))(first_weights)
         if 2 in stage or rsteps < 2:
             for a in (1, 2):
                 forward(a)
@@ -414,13 +426,12 @@
         spread(3, 2)
 
     for k, (n, cond) in enumerate(groups):
+        if k == max(0, len(groups) - 2) and nj > 2:
+            pl.when(jnp.logical_not(early))(spread_two)
         arrive(xr.at[pl.ds(0, (np_ - 1) * n)], x_r.at[k], cond)
 
-    if nj > 2:
-        pl.when(jnp.logical_not(early))(spread_two)
-
     for b in range(2):
-        for e in list(range(1, ny)) + [0]:
+        for e in far_y + [0]:
             row = 2 * lax.rem(y + e, ny) + b
             for j in range(nr):
                 o = lax.div(chosen[row, nloc + j], sb)
@@ -469,6 +480,7 @@
 
     lax.fori_loop(0, len(near) + 1, project_near, 0)
     flush(drains)
+    pl.when(jnp.logical_not(first_two))(pass_out)
     if nj > 2:
         for a in range(3):
             pass_on(a, 2)
@@ -505,7 +517,8 @@
             gain = hgs[h // 2, h % 2 : h % 2 + 1].astype(F32)
             ho[b * blk : (b + 1) * blk, h * 128 : (h + 1) * 128] = rms(v, gain).astype(BF16)
         if b == 0:
-            for j in range(nj):
+            pl.when(first_two)(pass_out)
+            for j in range(len(near), nj):
                 pass_on(3, j)
 
     own_cps[3].wait()
@@ -528,7 +541,7 @@
         out_cp(t).start()
         return 0
 
-    lax.fori_loop(0, tiles, finish, 0)
+    lax.fori_loop(0, tiles, finish, 0, unroll=True)
     flush(late)
     for t in range(tiles):
         out_cp(t).wait()

time: 53.9 us -> 52.9 us (0.981)
  Pallas kernels: 51.9 us -> 50.8 us
    pallas_call x1, Pallas kernels: 51.9 us -> 50.8 us  [body(): pl.pallas_call(functools.partial(kernel, dims), out_shape=jax.ShapeDtypeS...]
where the time goes in v4:
time: 52.9 us; the launch traced here: 52.7 us
  Pallas kernels  50.8 us (96%)
  local copies, waits for them, and re-layouts  1.88 us (4%)
    pallas_call x1, Pallas kernels, body(): pl.pallas_call(functools.partial(kernel, dims), out_shape=jax.ShapeDtypeS...  50.8 us
    unnamed x1, local copies, waits for them, and re-layouts  1.88 us

profile of v4, /device:TPU:1, one launch (start us, length us, event | category | flops | bytes accessed | tf_op | source)
XLA Modules:
  0.0 52.7 jit_solution(17281486822917870087)
XLA Ops:
  0.0 50.8 %attend.1 = bf16[128,2048]{1,0:T(8,128)(2,1)} custom-call(s32[8,16]{1,0:T(8,128)} %chosen_hbm.1, bf16[128,2048]{1,0:T(8,128)(2,1)} %tokens_hbm.1, bf16[2048,256]{1,0:T(8,128)(2,1)} %lw_hbm.1, bf16[2048,256]{1,0:T(8,128)(2,1)} %qw_hbm.1, bf16[256,256]{1,0:T(8,128)(2,1)} %bitcast.2, bf16[512,128]{1,0:T(8,128)(2,1)} %bitcast.3, bf16[256,2048]{1,0:T(8,128)(2,1)} %ow_hbm.1, ...), custom_call_target="tpu_custom_call" | custom-call | tf_op jit(solution)/shard_map/attend/pallas_call | solution.py:594
  50.8 1.9 %copy.12 = bf16[128,2048]{1,0:T(8,128)(2,1)} copy(bf16[128,2048]{1,0:T(8,128)(2,1)} %attend.1) | data formatting | bytes 1048576

commit v5 on v4

--- a/solution.py
+++ b/solution.py
@@ -103,33 +103,6 @@
             when(cond, cp.wait_send)
         queue.clear()
 
-    split = nz > 4
-    offsets = sorted({1 % nz, 2 % nz, (nz - 1) % nz, (nz - 2) % nz} - {0})
-    barrier = pltpu.get_barrier_semaphore()
-    peers = [(at_y(e), None) for e in range(1, ny)]
-    peers += [(at_z(d), z + d < nz if split and d < 3 else None) for d in offsets]
-    peers += [(at_plane(d), None) for d in range(1, np_)]
-
-    def greet(sem, dev):
-        pl.semaphore_signal(sem, inc=1, device_id=dev, device_id_type=MESH)
-
-    for dev, cond in peers:
-        when(cond, functools.partial(greet, barrier, dev))
-
-    def enter():
-        if not split:
-            pl.semaphore_wait(barrier, len(peers))
-            return
-        for k, cond in ((0, z >= 2), (1, z == 1), (2, z == 0)):
-            pl.when(cond)(functools.partial(pl.semaphore_wait, barrier, len(peers) - k))
-        for d in (1, 2):
-            pl.when(z + d >= nz)(functools.partial(greet, ready, at_z(d)))
-
-    def wait_wrap():
-        if split:
-            pl.when(z == 0)(functools.partial(pl.semaphore_wait, ready, 2))
-            pl.when(z == 1)(functools.partial(pl.semaphore_wait, ready, 1))
-
     tok_cp = pltpu.make_async_copy(tokens_hbm, tok, loc_sem.at[0])
     lw_cp = pltpu.make_async_copy(lw_hbm, lw, loc_sem.at[1])
     own_cps = [
@@ -144,8 +117,35 @@
         pltpu.make_async_copy(qg_hbm, qg, loc_sem.at[9]),
         pltpu.make_async_copy(hg, hgs.at[y], loc_sem.at[10]),
     ]
-    for cp in small_cps + [tok_cp, lw_cp]:
+    for cp in [tok_cp, lw_cp] + small_cps:
         cp.start()
+
+    split = nz > 4
+    offsets = sorted({1 % nz, 2 % nz, (nz - 1) % nz, (nz - 2) % nz} - {0})
+    barrier = pltpu.get_barrier_semaphore()
+    peers = [(at_y(e), None) for e in range(1, ny)]
+    peers += [(at_z(d), z + d < nz if split and d < 3 else None) for d in offsets]
+    peers += [(at_plane(d), None) for d in range(1, np_)]
+
+    def greet(sem, dev):
+        pl.semaphore_signal(sem, inc=1, device_id=dev, device_id_type=MESH)
+
+    for dev, cond in peers:
+        when(cond, functools.partial(greet, barrier, dev))
+
+    def enter():
+        if not split:
+            pl.semaphore_wait(barrier, len(peers))
+            return
+        for k, cond in ((0, z >= 2), (1, z == 1), (2, z == 0)):
+            pl.when(cond)(functools.partial(pl.semaphore_wait, barrier, len(peers) - k))
+        for d in (1, 2):
+            pl.when(z + d >= nz)(functools.partial(greet, ready, at_z(d)))
+
+    def wait_wrap():
+        if split:
+            pl.when(z == 0)(functools.partial(pl.semaphore_wait, ready, 2))
+            pl.when(z == 1)(functools.partial(pl.semaphore_wait, ready, 1))
 
     xs[...] = jnp.zeros_like(xs)
     xr[...] = jnp.zeros_like(xr)

time: 52.9 us -> 52.9 us (level)
  no operation moved by 1% of the time
where the time goes in v5:
time: 52.9 us; the launch traced here: 52.7 us
  Pallas kernels  50.8 us (96%)
  local copies, waits for them, and re-layouts  1.88 us (4%)
    pallas_call x1, Pallas kernels, body(): pl.pallas_call(functools.partial(kernel, dims), out_shape=jax.ShapeDtypeS...  50.8 us
    unnamed x1, local copies, waits for them, and re-layouts  1.88 us

profile of v5, /device:TPU:1, one launch (start us, length us, event | category | flops | bytes accessed | tf_op | source)
XLA Modules:
  0.0 52.7 jit_solution(4174110707681375231)
XLA Ops:
  0.0 50.8 %attend.1 = bf16[128,2048]{1,0:T(8,128)(2,1)} custom-call(s32[8,16]{1,0:T(8,128)} %chosen_hbm.1, bf16[128,2048]{1,0:T(8,128)(2,1)} %tokens_hbm.1, bf16[2048,256]{1,0:T(8,128)(2,1)} %lw_hbm.1, bf16[2048,256]{1,0:T(8,128)(2,1)} %qw_hbm.1, bf16[256,256]{1,0:T(8,128)(2,1)} %bitcast.2, bf16[512,128]{1,0:T(8,128)(2,1)} %bitcast.3, bf16[256,2048]{1,0:T(8,128)(2,1)} %ow_hbm.1, ...), custom_call_target="tpu_custom_call" | custom-call | tf_op jit(solution)/shard_map/attend/pallas_call | solution.py:594
  50.8 1.9 %copy.12 = bf16[128,2048]{1,0:T(8,128)(2,1)} copy(bf16[128,2048]{1,0:T(8,128)(2,1)} %attend.1) | data formatting | bytes 1048576
